TPU v7x, 32 devices: a whole 2x2x4 slice. The times are simulated.
32 devices in a mesh: grp: 2 (over y), sp: 4 (over z), tp: 4 (over x, core).
Axes of the slice: x: 2, y: 2, z: 4, core: 2. Of those that a mesh axis runs over, the one named last changes fastest.
Arguments:
- tokens: bfloat16 [8, 1024, 2048], P('grp', 'sp'), parts along dimension 0, may hold values from -6 to 6
- norm_gain: bfloat16 [2048], replicated, may hold values from 0.099609375 to 1.8984375
- key_weight: bfloat16 [2048, 2048], P(None, 'tp'), may hold values from -0.125 to 0.125
- value_weight: bfloat16 [2048, 2048], P(None, 'tp'), may hold values from -0.125 to 0.125
- break_bias: bfloat16 [8, 1024, 16], P('grp', 'sp', 'tp'), parts along dimension 0, may hold values from -12 to 0
- new_query: bfloat16 [8, 2048], P('grp', 'tp'), parts along dimension 0, may hold values from -6 to 6
Outputs:
- cache_pair: bfloat16 [8, 4, 256, 2, 2048], P(('grp', 'sp'), None, None, None, 'tp'), parts along dimension 0
- cache_bias: bfloat16 [8, 4, 256, 16], P(('grp', 'sp'), None, None, 'tp'), parts along dimension 0
- attended: float32 [8, 2048], P('grp', 'tp'), parts along dimension 0
There are 2 independent parts, one for each index of `grp`. A program takes and returns all parts, laid end to end along the dimension named above; an argument that names none is the same for every part. Nothing has to cross between parts.
All inputs are finite; a program needn't handle non-finite values.
Results may differ from a plain program's by a relative error of at most 0.0064.
Values may be sent and summed in bfloat16 or wider, within the bound.
No kernel may reach another device: no remote copies, remote signals or barrier semaphores. Data moves between devices by JAX's collectives and lax.ppermute only.
A program may use at most 64 MiB of HBM per device.

v0:
```python
import jax
import jax.numpy as jnp
from jax import lax
from jax.sharding import PartitionSpec as P

norm_eps = 1e-06


def normalize(tokens, norm_gain):
    widened = tokens.astype(jnp.float32)
    inverse = lax.rsqrt(jnp.mean(widened * widened, axis=-1, keepdims=True) + norm_eps)
    return (widened * inverse * norm_gain.astype(jnp.float32)).astype(jnp.bfloat16)


def project(flat_rows, key_weight, value_weight):
    key_rows = jnp.dot(flat_rows, key_weight, preferred_element_type=jnp.float32).astype(
        jnp.bfloat16
    )
    value_rows = jnp.dot(flat_rows, value_weight, preferred_element_type=jnp.float32).astype(
        jnp.bfloat16
    )
    return (key_rows, value_rows)


def read_placed(new_query, key_rows, value_rows, bias_rows, seq_count):
    block_count, piece, heads_here = bias_rows.shape
    columns = key_rows.shape[2]
    head_size = columns // heads_here
    span = block_count // seq_count
    own_index = lax.axis_index("sp")
    own_seq = own_index // span
    own_part = own_index % span
    own_query = lax.dynamic_slice_in_dim(new_query, own_seq, 1, 0).reshape(heads_here, head_size)
    key_heads = key_rows.reshape(block_count, piece, heads_here, head_size)
    logits = jnp.einsum("hd,nphd->nph", own_query, key_heads, preferred_element_type=jnp.float32)
    logits = logits * head_size ** (-0.5) + bias_rows.astype(jnp.float32)
    keep_log = jax.nn.log_sigmoid(-logits)
    block_totals = jnp.sum(keep_log, axis=1)
    own_slot = (jnp.arange(block_count, dtype=jnp.int32) == own_index)[:, None, None]
    placed = jnp.where(own_slot, block_totals[None], 0.0)
    gathered = lax.psum(placed, "sp")
    same_prompt = lax.dynamic_slice_in_dim(gathered, own_seq * span, span, 0)
    ordered = jnp.transpose(same_prompt, (1, 0, 2)).reshape(block_count * span, heads_here)
    beyond = lax.cumsum(ordered, axis=0, reverse=True) - ordered
    beyond = beyond.reshape(block_count, span, heads_here)
    carried = lax.dynamic_slice_in_dim(beyond, own_part, 1, 1)[:, 0, :]
    later_sum = lax.cumsum(keep_log, axis=1, reverse=True) - keep_log + carried[:, None, :]
    stick_weights = jnp.exp(jax.nn.log_sigmoid(logits) + later_sum).astype(jnp.bfloat16)
    value_heads = value_rows.reshape(block_count, piece, heads_here, head_size)
    mixed = jnp.einsum(
        "nph,nphd->hd", stick_weights, value_heads, preferred_element_type=jnp.float32
    )
    chosen = (jnp.arange(seq_count, dtype=jnp.int32) == own_seq)[:, None]
    partial_rows = jnp.where(chosen, mixed.reshape(1, columns), 0.0)
    return lax.psum(partial_rows, "sp")


def local(tokens, norm_gain, key_weight, value_weight, break_bias, new_query):
    seq_count, tok_rows, width = tokens.shape
    heads_here = break_bias.shape[2]
    block_count = lax.axis_size("sp")
    piece = tok_rows * seq_count // block_count
    columns = key_weight.shape[1]
    normed = normalize(tokens, norm_gain)
    bias_pieces = break_bias.reshape(block_count, piece, heads_here)
    key_rows, value_rows = project(normed.reshape(-1, width), key_weight, value_weight)
    stacked_rows = jnp.stack((key_rows, value_rows), axis=1).reshape(block_count, piece, 2, columns)
    paired, bias_arrived = (
        lax.all_to_all(stacked_rows, "sp", split_axis=0, concat_axis=0, tiled=True),
        lax.all_to_all(bias_pieces, "sp", split_axis=0, concat_axis=0, tiled=True),
    )
    key_rows = paired[:, :, 0]
    value_rows = paired[:, :, 1]
    attended = read_placed(new_query, key_rows, value_rows, bias_arrived, seq_count)
    return (paired[None], bias_arrived[None], attended)


def solution(mesh):
    return jax.shard_map(
        local,
        mesh=mesh,
        in_specs=(
            P("grp", "sp", None),
            P(),
            P(None, "tp"),
            P(None, "tp"),
            P("grp", "sp", "tp"),
            P("grp", "tp"),
        ),
        out_specs=(
            P(("grp", "sp"), None, None, None, "tp"),
            P(("grp", "sp"), None, None, "tp"),
            P("grp", "tp"),
        ),
        check_vma=False,
    )
```

profile of v0, /device:TPU:0, one launch (start us, length us, event | category | flops | bytes accessed | tf_op | source)
XLA Modules:
  0.0 130.2 jit_solution(2703418311215314435)
XLA Ops:
  0.7 6.5 %all-to-all-start.1 = ((bf16[4,256,4]{1,2,0:T(4,128)(2,1)}), bf16[4,256,4]{1,2,0:T(4,128)(2,1)S(1)}, u32[]{:S(2)}, u32[]{:S(2)}) async-start(bf16[4,256,4]{1,2,0:T(4,128)(2,1)} %param.10), calls=%async_computation.1 | async-start | bytes 16384 | tf_op jit(solution)/shard_map/all_to_all | solution.py:70
  7.1 3.2 %fusion = f32[4,256]{1,0:T(4,128)S(1)} fusion(bf16[4,256,2048]{2,1,0:T(8,128)(2,1)} %param.6), kind=kLoop, calls=%fused_computation.2 | loop fusion | flops 6290432 | bytes 4198400 | tf_op jit(solution)/shard_map/reduce_sum | solution.py:11
  10.4 0.2 copy-done.1
  10.6 1.0 fusion.2
  11.6 3.3 %convolution_convert_fusion.1 = bf16[1024,512]{1,0:T(8,128)(2,1)} fusion(bf16[1024,2048]{1,0:T(8,128)(2,1)S(1)} %bitcast.69, bf16[2048,512]{1,0:T(8,128)(2,1)S(1)} %copy-done), kind=kOutput, calls=%fused_computation.7 | convolution fusion | flops 2148007936 | bytes 7340032 | tf_op jit(solution)/shard_map/dot_general | solution.py:16
  15.0 1.5 %copy.18 = bf16[4,256,1,512]{1,3,2,0:T(8,128)(2,1)S(1)} copy(bf16[4,256,1,512]{3,1,0,2:T(8,128)(2,1)} %bitcast.72) | data formatting | bytes 2097152 | tf_op jit(solution)/shard_map/stack | solution.py:67
  16.4 6.2 %convolution_convert_fusion = bf16[1024,512]{1,0:T(8,128)(2,1)} fusion(bf16[1024,2048]{1,0:T(8,128)(2,1)} %bitcast.70, bf16[2048,512]{1,0:T(8,128)(2,1)} %param.9), kind=kOutput, calls=%fused_computation.6 | convolution fusion | flops 2148007936 | bytes 7340032 | tf_op jit(solution)/shard_map/dot_general | solution.py:19
  22.6 2.3 %copy.19 = bf16[4,256,1,512]{1,3,2,0:T(8,128)(2,1)} copy(bf16[4,256,1,512]{3,1,0,2:T(8,128)(2,1)} %bitcast.71) | data formatting | bytes 2097152 | tf_op jit(solution)/shard_map/stack | solution.py:67
  24.9 2.7 %pad_maximum_fusion = bf16[4,256,2,512]{1,3,2,0:T(8,128)(2,1)} fusion(bf16[4,256,1,512]{1,3,2,0:T(8,128)(2,1)} %copy.19, bf16[4,256,1,512]{1,3,2,0:T(8,128)(2,1)S(1)} %copy.18), kind=kLoop, calls=%fused_computation.5 | loop fusion | flops 1048576 | bytes 4194304 | tf_op jit(solution)/shard_map/stack | solution.py:67
  27.6 5.2 %all-to-all-start = ((bf16[4,256,2,512]{1,3,2,0:T(8,128)(2,1)}), bf16[4,256,2,512]{1,3,2,0:T(8,128)(2,1)}, u32[]{:S(2)}, u32[]{:S(2)}) async-start(bf16[4,256,2,512]{1,3,2,0:T(8,128)(2,1)} %pad_maximum_fusion), calls=%async_computation | async-start | bytes 4194304 | tf_op jit(solution)/shard_map/all_to_all | solution.py:69
  32.8 47.8 %all-to-all-done = bf16[4,256,2,512]{1,3,2,0:T(8,128)(2,1)} async-done(((bf16[4,256,2,512]{1,3,2,0:T(8,128)(2,1)}), bf16[4,256,2,512]{1,3,2,0:T(8,128)(2,1)}, u32[]{:S(2)}, u32[]{:S(2)}) %all-to-all-start) | async-done | bytes 2097184 | tf_op jit(solution)/shard_map/all_to_all | solution.py:69
  80.6 1.7 %fusion.20 = (bf16[4,256,1,512]{1,3,2,0:T(8,128)(2,1)S(1)}, bf16[4,256,1,512]{1,3,2,0:T(8,128)(2,1)S(1)}) fusion(bf16[4,256,2,512]{1,3,2,0:T(8,128)(2,1)} %all-to-all-done), kind=kLoop, calls=%fused_computation.37 | loop fusion | bytes 4194304 | tf_op jit(solution)/shard_map/slice | solution.py:72
  82.3 0.2 fusion.5
  82.5 0.1 negate_bitcast_fusion
  82.7 10.0 %psum.14 = f32[4,4,4]{2,1,0:T(4,128)S(1)} all-reduce(f32[4,4,4]{2,1,0:T(4,128)S(1)} %broadcast_select_fusion.1), channel_id=1, replica_groups=mesh['grp'=2,'sp'=4,'tp'=4] {'sp'}, use_global_device_ids=true, to_apply=%region_4.5 | all-reduce | flops 64 | bytes 512 | tf_op jit(solution)/shard_map/psum | solution.py:41
  92.8 20.1 %reduce-window.6 = f32[4,4,2,128]{3,2,1,0:T(2,128)S(1)} reduce-window(f32[4,4,2,128]{3,2,1,0:T(2,128)S(1)} %reshape.54, f32[]{:T(128)} %constant.36.clone.1), window={size=1x1x1x128 pad=0_0x0_0x0_0x0_127}, to_apply=%region_1.2 | reduce-window | flops 520192 | bytes 32772 | tf_op jit(solution)/shard_map/reduce-window
  112.9 0.1 copy.21
  113.1 0.1 copy.22
  113.2 0.1 broadcast_add_fusion
  113.3 0.1 fusion.13
  113.4 0.4 fusion.3
  113.8 9.6 %psum.15 = f32[4,512]{1,0:T(4,128)} all-reduce(f32[4,512]{1,0:T(4,128)S(1)} %broadcast_select_fusion), channel_id=1, replica_groups=mesh['grp'=2,'sp'=4,'tp'=4] {'sp'}, use_global_device_ids=true, to_apply=%region_6.7 | all-reduce | flops 2048 | bytes 16384 | tf_op jit(solution)/shard_map/psum | solution.py:55
  123.5 6.2 %copy.24 = bf16[1,4,256,2,512]{4,3,2,1,0:T(2,128)(2,1)} copy(bf16[1,4,256,2,512]{2,4,3,1,0:T(8,128)(2,1)} %bitcast.3) | data formatting | bytes 4194304
  129.6 0.6 copy.51
  (23 shorter events, 0.3 us)
Async XLA Ops:
  0.6 11.0 %copy-start = (bf16[2048,512]{1,0:T(8,128)(2,1)S(1)}, bf16[2048,512]{1,0:T(8,128)(2,1)}, u32[]{:S(2)}) copy-start(bf16[2048,512]{1,0:T(8,128)(2,1)} %param.8) | copy-start | bytes 6291460
  0.6 9.7 %copy-start.3 = (bf16[2048]{0:T(1024)(128)(2,1)S(1)}, bf16[2048]{0:T(1024)(128)(2,1)}, u32[]{:S(2)}) copy-start(bf16[2048]{0:T(1024)(128)(2,1)} %param.7) | copy-start | bytes 12292
  0.7 27.0 %all-to-all-start.1 = ((bf16[4,256,4]{1,2,0:T(4,128)(2,1)}), bf16[4,256,4]{1,2,0:T(4,128)(2,1)S(1)}, u32[]{:S(2)}, u32[]{:S(2)}) async-start(bf16[4,256,4]{1,2,0:T(4,128)(2,1)} %param.10), calls=%async_computation.1 | async-start | bytes 16384 | tf_op jit(solution)/shard_map/all_to_all | solution.py:70
  7.1 3.4 %copy-start.1 = (bf16[4,256,2048]{2,1,0:T(8,128)(2,1)S(1)}, bf16[4,256,2048]{2,1,0:T(8,128)(2,1)}, u32[]{:S(2)}) copy-start(bf16[4,256,2048]{2,1,0:T(8,128)(2,1)} %param.6) | copy-start | bytes 12582916
  11.6 3.3 %copy-start.2 = (bf16[4,256,2048]{2,1,0:T(8,128)(2,1)}, bf16[4,256,2048]{2,1,0:T(8,128)(2,1)S(1)}, u32[]{:S(2)}) copy-start(bf16[4,256,2048]{2,1,0:T(8,128)(2,1)S(1)} %fusion.2) | copy-start | bytes 12582916
  27.6 54.7 %copy-start.4 = (bf16[4,512]{1,0:T(4,128)(2,1)S(1)}, bf16[4,512]{1,0:T(4,128)(2,1)}, u32[]{:S(2)}) copy-start(bf16[4,512]{1,0:T(4,128)(2,1)} %param.11) | copy-start | bytes 12292
  27.6 53.0 %all-to-all-start = ((bf16[4,256,2,512]{1,3,2,0:T(8,128)(2,1)}), bf16[4,256,2,512]{1,3,2,0:T(8,128)(2,1)}, u32[]{:S(2)}, u32[]{:S(2)}) async-start(bf16[4,256,2,512]{1,3,2,0:T(8,128)(2,1)} %pad_maximum_fusion), calls=%async_computation | async-start | bytes 4194304 | tf_op jit(solution)/shard_map/all_to_all | solution.py:69
where the time goes:
time: 131 us; the launch traced here: 130 us
  waiting for transfers between devices  47.8 us (36%)
  other arithmetic  27.6 us (21%)
  blocking collectives  19.6 us (15%)
  local copies, waits for them, and re-layouts  12.7 us (10%)
  starting transfers between devices  11.7 us (9%)
  matrix products  10.1 us (8%)
    all_to_all x1, waiting for transfers between devices, local(): lax.all_to_all(stacked_rows, 'sp', split_axis=0, concat_axis=0, tiled=True)  47.8 us
    another operation x2, other arithmetic  20.1 us
    psum x1, blocking collectives, read_placed(): gathered = lax.psum(placed, 'sp')  9.95 us
    psum x1, blocking collectives, read_placed(): return lax.psum(partial_rows, 'sp')  9.64 us
    unnamed x12, local copies, waits for them, and re-layouts  6.96 us
    all_to_all x1, starting transfers between devices, local(): lax.all_to_all(bias_pieces, 'sp', split_axis=0, concat_axis=0, tiled=True)  6.49 us
    dot_general x1, matrix products, project(): jnp.dot(flat_rows, value_weight, preferred_element_type=jnp.float32)  6.16 us
    all_to_all x1, starting transfers between devices, local(): lax.all_to_all(stacked_rows, 'sp', split_axis=0, concat_axis=0, tiled=True)  5.22 us
  transfers between devices with their start and end apart: 2, of which 1 were waited for; matrix products, arithmetic and copies ran while one was open for 16% of the time, Pallas kernels for 0%

commit v1 on v0

--- a/solution.py
+++ b/solution.py
@@ -38,7 +38,8 @@
     block_totals = jnp.sum(keep_log, axis=1)
     own_slot = (jnp.arange(block_count, dtype=jnp.int32) == own_index)[:, None, None]
     placed = jnp.where(own_slot, block_totals[None], 0.0)
-    gathered = lax.psum(placed, "sp")
+    parts = lax.all_gather(placed, "sp")
+    gathered = jnp.sum(parts, axis=0)
     same_prompt = lax.dynamic_slice_in_dim(gathered, own_seq * span, span, 0)
     ordered = jnp.transpose(same_prompt, (1, 0, 2)).reshape(block_count * span, heads_here)
     beyond = lax.cumsum(ordered, axis=0, reverse=True) - ordered

time: 131 us -> 135 us (1.031)
  blocking collectives: 19.6 us -> 23.7 us
    all_gather x0 -> x1, blocking collectives: none -> 13.1 us  [read_placed(): parts = lax.all_gather(placed, 'sp')]
    psum x1 -> x0, blocking collectives: 9.95 us -> none  [read_placed(): gathered = lax.psum(placed, 'sp')]
  transfers between devices with their start and end apart: 2 -> 2, of which waited for: 1 -> 1; matrix products, arithmetic and copies ran while one was open for 16% -> 15% of each run, Pallas kernels for 0% -> 0%
where the time goes in v1:
time: 135 us; the launch traced here: 134 us
  waiting for transfers between devices  47.8 us (35%)
  other arithmetic  27.6 us (20%)
  blocking collectives  23.7 us (18%)
  local copies, waits for them, and re-layouts  12.7 us (9%)
  starting transfers between devices  11.7 us (9%)
  matrix products  10.1 us (7%)
    all_to_all x1, waiting for transfers between devices, local(): lax.all_to_all(stacked_rows, 'sp', split_axis=0, concat_axis=0, tiled=True)  47.8 us
    another operation x2, other arithmetic  20.1 us
    all_gather x1, blocking collectives, read_placed(): parts = lax.all_gather(placed, 'sp')  13.1 us
    psum x1, blocking collectives, read_placed(): return lax.psum(partial_rows, 'sp')  10.6 us
    unnamed x12, local copies, waits for them, and re-layouts  6.96 us
    all_to_all x1, starting transfers between devices, local(): lax.all_to_all(bias_pieces, 'sp', split_axis=0, concat_axis=0, tiled=True)  6.49 us
    dot_general x1, matrix products, project(): jnp.dot(flat_rows, value_weight, preferred_element_type=jnp.float32)  6.16 us
    all_to_all x1, starting transfers between devices, local(): lax.all_to_all(stacked_rows, 'sp', split_axis=0, concat_axis=0, tiled=True)  5.22 us
  transfers between devices with their start and end apart: 2, of which 1 were waited for; matrix products, arithmetic and copies ran while one was open for 15% of the time, Pallas kernels for 0%

profile of v1, /device:TPU:0, one launch (start us, length us, event | category | flops | bytes accessed | tf_op | source)
XLA Modules:
  0.0 134.3 jit_solution(3318801790928387108)
XLA Ops:
  0.7 6.5 %all-to-all-start.1 = ((bf16[4,256,4]{1,2,0:T(4,128)(2,1)}), bf16[4,256,4]{1,2,0:T(4,128)(2,1)S(1)}, u32[]{:S(2)}, u32[]{:S(2)}) async-start(bf16[4,256,4]{1,2,0:T(4,128)(2,1)} %param.10), calls=%async_computation.1 | async-start | bytes 16384 | tf_op jit(solution)/shard_map/all_to_all | solution.py:71
  7.1 3.2 %fusion = f32[4,256]{1,0:T(4,128)S(1)} fusion(bf16[4,256,2048]{2,1,0:T(8,128)(2,1)} %param.6), kind=kLoop, calls=%fused_computation.2 | loop fusion | flops 6290432 | bytes 4198400 | tf_op jit(solution)/shard_map/reduce_sum | solution.py:11
  10.4 0.2 copy-done.1
  10.6 1.0 fusion.2
  11.6 3.3 %convolution_convert_fusion.1 = bf16[1024,512]{1,0:T(8,128)(2,1)} fusion(bf16[1024,2048]{1,0:T(8,128)(2,1)S(1)} %bitcast.69, bf16[2048,512]{1,0:T(8,128)(2,1)S(1)} %copy-done), kind=kOutput, calls=%fused_computation.7 | convolution fusion | flops 2148007936 | bytes 7340032 | tf_op jit(solution)/shard_map/dot_general | solution.py:16
  15.0 1.5 %copy.18 = bf16[4,256,1,512]{1,3,2,0:T(8,128)(2,1)S(1)} copy(bf16[4,256,1,512]{3,1,0,2:T(8,128)(2,1)} %bitcast.72) | data formatting | bytes 2097152 | tf_op jit(solution)/shard_map/stack | solution.py:68
  16.4 6.2 %convolution_convert_fusion = bf16[1024,512]{1,0:T(8,128)(2,1)} fusion(bf16[1024,2048]{1,0:T(8,128)(2,1)} %bitcast.70, bf16[2048,512]{1,0:T(8,128)(2,1)} %param.9), kind=kOutput, calls=%fused_computation.6 | convolution fusion | flops 2148007936 | bytes 7340032 | tf_op jit(solution)/shard_map/dot_general | solution.py:19
  22.6 2.3 %copy.19 = bf16[4,256,1,512]{1,3,2,0:T(8,128)(2,1)} copy(bf16[4,256,1,512]{3,1,0,2:T(8,128)(2,1)} %bitcast.71) | data formatting | bytes 2097152 | tf_op jit(solution)/shard_map/stack | solution.py:68
  24.9 2.7 %pad_maximum_fusion = bf16[4,256,2,512]{1,3,2,0:T(8,128)(2,1)} fusion(bf16[4,256,1,512]{1,3,2,0:T(8,128)(2,1)} %copy.19, bf16[4,256,1,512]{1,3,2,0:T(8,128)(2,1)S(1)} %copy.18), kind=kLoop, calls=%fused_computation.5 | loop fusion | flops 1048576 | bytes 4194304 | tf_op jit(solution)/shard_map/stack | solution.py:68
  27.6 5.2 %all-to-all-start = ((bf16[4,256,2,512]{1,3,2,0:T(8,128)(2,1)}), bf16[4,256,2,512]{1,3,2,0:T(8,128)(2,1)}, u32[]{:S(2)}, u32[]{:S(2)}) async-start(bf16[4,256,2,512]{1,3,2,0:T(8,128)(2,1)} %pad_maximum_fusion), calls=%async_computation | async-start | bytes 4194304 | tf_op jit(solution)/shard_map/all_to_all | solution.py:70
  32.8 47.8 %all-to-all-done = bf16[4,256,2,512]{1,3,2,0:T(8,128)(2,1)} async-done(((bf16[4,256,2,512]{1,3,2,0:T(8,128)(2,1)}), bf16[4,256,2,512]{1,3,2,0:T(8,128)(2,1)}, u32[]{:S(2)}, u32[]{:S(2)}) %all-to-all-start) | async-done | bytes 2097184 | tf_op jit(solution)/shard_map/all_to_all | solution.py:70
  80.6 1.7 %fusion.20 = (bf16[4,256,1,512]{1,3,2,0:T(8,128)(2,1)S(1)}, bf16[4,256,1,512]{1,3,2,0:T(8,128)(2,1)S(1)}) fusion(bf16[4,256,2,512]{1,3,2,0:T(8,128)(2,1)} %all-to-all-done), kind=kLoop, calls=%fused_computation.37 | loop fusion | bytes 4194304 | tf_op jit(solution)/shard_map/slice | solution.py:73
  82.3 0.2 fusion.5
  82.5 0.1 negate_bitcast_fusion
  82.7 13.1 %all_gather.4 = f32[4,4,4,4]{3,2,1,0:T(4,128)S(1)} all-gather(f32[1,4,4,4]{3,2,1,0:T(4,128)S(1)} %broadcast_select_fusion.1), channel_id=1, replica_groups=mesh['grp'=2,'sp'=4,'tp'=4] {'sp'}, dimensions={0}, use_global_device_ids=true | all-gather | bytes 1280 | tf_op jit(solution)/shard_map/all_gather | solution.py:41
  96.0 20.1 %reduce-window.6 = f32[4,4,2,128]{3,2,1,0:T(2,128)S(1)} reduce-window(f32[4,4,2,128]{3,2,1,0:T(2,128)S(1)} %reshape.57, f32[]{:T(128)} %constant.36.clone.1), window={size=1x1x1x128 pad=0_0x0_0x0_0x0_127}, to_apply=%region_1.2 | reduce-window | flops 520192 | bytes 32772 | tf_op jit(solution)/shard_map/reduce-window
  116.1 0.1 copy.21
  116.3 0.1 copy.22
  116.4 0.1 broadcast_add_fusion
  116.5 0.1 fusion.13
  116.6 0.4 fusion.3
  117.0 10.6 %psum.7 = f32[4,512]{1,0:T(4,128)} all-reduce(f32[4,512]{1,0:T(4,128)S(1)} %broadcast_select_fusion), channel_id=1, replica_groups=mesh['grp'=2,'sp'=4,'tp'=4] {'sp'}, use_global_device_ids=true, to_apply=%region_6.7 | all-reduce | flops 2048 | bytes 16384 | tf_op jit(solution)/shard_map/psum | solution.py:56
  127.6 6.2 %copy.24 = bf16[1,4,256,2,512]{4,3,2,1,0:T(2,128)(2,1)} copy(bf16[1,4,256,2,512]{2,4,3,1,0:T(8,128)(2,1)} %bitcast.3) | data formatting | bytes 4194304
  133.7 0.6 copy.51
  (24 shorter events, 0.3 us)
Async XLA Ops:
  0.6 11.0 %copy-start = (bf16[2048,512]{1,0:T(8,128)(2,1)S(1)}, bf16[2048,512]{1,0:T(8,128)(2,1)}, u32[]{:S(2)}) copy-start(bf16[2048,512]{1,0:T(8,128)(2,1)} %param.8) | copy-start | bytes 6291460
  0.6 9.7 %copy-start.3 = (bf16[2048]{0:T(1024)(128)(2,1)S(1)}, bf16[2048]{0:T(1024)(128)(2,1)}, u32[]{:S(2)}) copy-start(bf16[2048]{0:T(1024)(128)(2,1)} %param.7) | copy-start | bytes 12292
  0.7 27.0 %all-to-all-start.1 = ((bf16[4,256,4]{1,2,0:T(4,128)(2,1)}), bf16[4,256,4]{1,2,0:T(4,128)(2,1)S(1)}, u32[]{:S(2)}, u32[]{:S(2)}) async-start(bf16[4,256,4]{1,2,0:T(4,128)(2,1)} %param.10), calls=%async_computation.1 | async-start | bytes 16384 | tf_op jit(solution)/shard_map/all_to_all | solution.py:71
  7.1 3.4 %copy-start.1 = (bf16[4,256,2048]{2,1,0:T(8,128)(2,1)S(1)}, bf16[4,256,2048]{2,1,0:T(8,128)(2,1)}, u32[]{:S(2)}) copy-start(bf16[4,256,2048]{2,1,0:T(8,128)(2,1)} %param.6) | copy-start | bytes 12582916
  11.6 3.3 %copy-start.2 = (bf16[4,256,2048]{2,1,0:T(8,128)(2,1)}, bf16[4,256,2048]{2,1,0:T(8,128)(2,1)S(1)}, u32[]{:S(2)}) copy-start(bf16[4,256,2048]{2,1,0:T(8,128)(2,1)S(1)} %fusion.2) | copy-start | bytes 12582916
  27.6 54.7 %copy-start.4 = (bf16[4,512]{1,0:T(4,128)(2,1)S(1)}, bf16[4,512]{1,0:T(4,128)(2,1)}, u32[]{:S(2)}) copy-start(bf16[4,512]{1,0:T(4,128)(2,1)} %param.11) | copy-start | bytes 12292
  27.6 53.0 %all-to-all-start = ((bf16[4,256,2,512]{1,3,2,0:T(8,128)(2,1)}), bf16[4,256,2,512]{1,3,2,0:T(8,128)(2,1)}, u32[]{:S(2)}, u32[]{:S(2)}) async-start(bf16[4,256,2,512]{1,3,2,0:T(8,128)(2,1)} %pad_maximum_fusion), calls=%async_computation | async-start | bytes 4194304 | tf_op jit(solution)/shard_map/all_to_all | solution.py:70
